TPU v7x, 256 devices: a whole 4x4x8 slice. The times are simulated.
256 devices in a mesh: sp: 64 (over z, x, core), tp: 4 (over y).
Axes of the slice: x: 4, y: 4, z: 8, core: 2. Of those that a mesh axis runs over, the one named last changes fastest.
Arguments:
- skip_connection_stream: bfloat16 [49152, 2048], P('sp'), may hold values from -6 to 6
- probing_vectors: bfloat16 [49152, 512], P('sp', 'tp'), may hold values from -6 to 6
- addressing_vectors: bfloat16 [49152, 512], P('sp', 'tp'), may hold values from -6 to 6
- mapped_payloads: bfloat16 [49152, 1024], P('sp', 'tp'), may hold values from -6 to 6
- emission_switch: bfloat16 [49152, 1024], P('sp', 'tp'), may hold values from -6 to 6
- lapse_preactivation: bfloat16 [49152, 512], P('sp', 'tp')
- lapse_shift_entries: float32 [512], P('tp')
- surplus_attenuation_terms: float32 [49152], P('sp'), may hold values from -0.7 to 0
- passage_label_per_token: int32 [49152], P('sp'), may hold values from 0 to 15, never falling along the last dimension, each value on 1 to 6144 neighbouring positions
- attention_group_rescaler: float32 [128], replicated, may hold values from 0.1 to 1.9
- emission_projector: bfloat16 [1024, 2048], P('tp'), may hold values from -0.1875 to 0.1875
- perceptron_rescaler: float32 [2048], replicated, may hold values from 0.1 to 1.9
- switching_projector: bfloat16 [2048, 5632], P('sp', 'tp'), may hold values from -0.125 to 0.125
- widening_projector: bfloat16 [2048, 5632], P('sp', 'tp'), may hold values from -0.125 to 0.125
- shrinking_projector: bfloat16 [5632, 2048], P('tp', 'sp'), may hold values from -0.078125 to 0.078125
Outputs:
- layer_out: bfloat16 [49152, 2048], P(('sp', 'tp'))
Inputs may be any that keep to these rules, and one draw needn't show every extreme that they name: `passage_label_per_token`: document numbers never fall along the sequence; a document holds at most 6144 positions.
All inputs are finite; a program needn't handle non-finite values.
Results may differ from a plain program's by a relative error of at most 0.014.
Values may be sent and summed in bfloat16 or wider, within the bound.
A program may use at most 128 MiB of HBM per device.

v0:
```python
import jax
import jax.numpy as jnp
from jax import lax
from jax.sharding import Mesh
from jax.sharding import PartitionSpec as P

DK = 64
DV = 128
BLOCK = 64
SP = ("sp_0", "sp_1", "sp_2")
SP_TP = ("sp_0", "sp_1", "sp_2", "tp")


eps = 1e-06
sharpness_factor = 16.0


def sent_together(arrays, axis, dim, along):
    ends, at = ([], 0)
    for a in arrays[:-1]:
        at += a.shape[along]
        ends.append(at)
    both = jnp.concatenate(arrays, axis=along)
    return tuple(jnp.split(lax.all_gather(both, axis, axis=dim, tiled=True), ends, axis=along))


def joined_along(parts, dim):
    parts = jnp.moveaxis(parts, 0, dim)
    lengths = parts.shape
    return parts.reshape(*lengths[:dim], lengths[dim] * lengths[dim + 1], *lengths[dim + 2 :])


def all_blocks(shard, axes, order):
    parts = shard
    for k in order:
        parts = lax.all_gather(parts, axes[k])
    done = order[::-1]
    back = [done.index(k) for k in range(len(axes))]
    parts = parts.transpose(*back, *range(len(axes), parts.ndim))
    return parts.reshape(-1, *shard.shape)


def whole_of(shard, axes, order, dim):
    return joined_along(all_blocks(shard, axes, order), dim)


def neutral_like(shard, identity):
    return jax.tree.map(
        lambda part, zero: jnp.zeros_like(part) + jnp.asarray(zero, part.dtype), shard, identity
    )


def collected_together(shard, axis):
    leaves = jax.tree.leaves(shard)
    order = sorted(range(len(leaves)), key=lambda k: -leaves[k].size)
    width = (1, *leaves[order[0]].shape)[-1]
    lines = [
        jnp.pad(leaves[k].reshape(-1), (0, -leaves[k].size % width)).reshape(-1, width)
        for k in order
    ]
    both, at, found = (lax.all_gather(jnp.concatenate(lines), axis), 0, {})
    for k, line in zip(order, lines):
        slab = both[:, at : at + len(line)].reshape(len(both), -1)
        found[k] = slab[:, : leaves[k].size].reshape(-1, *leaves[k].shape)
        at += len(line)
    numbers = iter(range(len(leaves)))
    return jax.tree.map(lambda _: found[next(numbers)], shard)


def carried_in(shard, axes, combine, identity):
    before = start = neutral_like(shard, identity)
    so_far = shard
    for axis in reversed(axes):
        size, place = (lax.axis_size(axis), lax.axis_index(axis))
        pieces = collected_together(
            jax.tree.map(
                lambda part, kind: part.astype(kind),
                so_far,
                jax.tree.map(lambda a: jnp.bfloat16 if a.dtype == jnp.float32 else a.dtype, shard),
            ),
            axis,
        )
        inside, so_far = (start, start)
        for k in range(size):
            passed = k < place
            so_far = combine(
                so_far, jax.tree.map(lambda part, own: part[k].astype(own.dtype), pieces, shard)
            )
            inside = jax.tree.map(lambda new, old: jnp.where(passed, new, old), so_far, inside)
        before = combine(inside, before)
    return before


def in_blocks(shard, dim, size):
    before, after = (shard.shape[:dim], shard.shape[dim + 1 :])
    return jnp.moveaxis(shard.reshape(*before, size, -1, *after), dim, 0)


def sum_at_owner(shard, axis, dim):
    size = lax.axis_size(axis)
    parts = lax.all_to_all(in_blocks(shard, dim, size), axis, 0, 0, tiled=True)
    return jnp.sum(parts.astype(jnp.float32), axis=0)


def head_split(array, heads):
    return array.reshape(array.shape[0], heads, -1).transpose(1, 0, 2)


def block_pass(
    query_head_rows,
    key_heads,
    value_heads,
    decay_heads,
    documents,
    recurrent_state,
    last_doc,
    offset,
    span,
):
    heads, length, _ = query_head_rows.shape
    blocks = length // span
    middle = span // 2

    def to_blocks(array):
        return array.reshape(heads, blocks, span, array.shape[-1]).transpose(1, 0, 2, 3)

    lower = jnp.tril(jnp.ones((span, span), dtype=bool))

    def step(carry, inputs):
        recurrent_state, last_doc, offset = carry
        query_block, key_blk, value_block, piece_attenuation, doc_blk = inputs
        cumulative_decay = jnp.cumsum(piece_attenuation, axis=1)
        previous_valid = (doc_blk == last_doc).astype(jnp.float32)
        cross_block_output = (
            jnp.einsum("gfl,glm->gfm", query_block * jnp.exp(cumulative_decay), recurrent_state)
            * previous_valid[None, :, None]
        )
        centre = cumulative_decay[:, middle : middle + 1, :]
        query_scaled = query_block * jnp.exp(cumulative_decay - centre)
        key_scaled = key_blk * jnp.exp(centre - cumulative_decay)
        same = (doc_blk[:, None] == doc_blk[None, :]) & lower
        raw_scores = jnp.einsum("hik,hjk->hij", query_scaled, key_scaled)
        scores = jnp.where(same[None, :, :], raw_scores, 0.0)
        result = cross_block_output + jnp.einsum("hij,hjv->hiv", scores, value_block)
        final_memory_summary = cumulative_decay[:, -1, :]
        last_valid = (doc_blk[-1] == last_doc).astype(jnp.float32)
        tail_ok = (doc_blk == doc_blk[-1]).astype(jnp.float32)
        decayed_keys = (
            key_blk
            * jnp.exp(final_memory_summary[:, None, :] - cumulative_decay)
            * tail_ok[None, :, None]
        )
        recurrent_state = recurrent_state * jnp.exp(final_memory_summary)[
            :, :, None
        ] * last_valid + jnp.einsum("wrz,wrs->wzs", decayed_keys, value_block)
        return (
            (recurrent_state, doc_blk[-1], offset + final_memory_summary),
            (result, cumulative_decay + offset[:, None, :]),
        )

    carry, outputs = lax.scan(
        step,
        (recurrent_state, last_doc, offset),
        (
            to_blocks(query_head_rows),
            to_blocks(key_heads),
            to_blocks(value_heads),
            to_blocks(decay_heads),
            documents.reshape(blocks, span),
        ),
    )
    result, running_state = outputs
    result = result.transpose(1, 0, 2, 3).reshape(heads, length, -1)
    running_state = running_state.transpose(1, 0, 2, 3).reshape(heads, length, -1)
    return (carry[0], carry[2], result, running_state)


def join_spans(earlier, later):
    linked = ((earlier[3] == later[2]) | (earlier[3] < 0.0) | (later[2] < 0.0)).astype(jnp.float32)
    decay_total = earlier[0] * later[0] * linked
    state_total = earlier[1] * (later[0] * linked)[:, :, None] + later[1]
    first_doc = jnp.where(earlier[2] < 0.0, later[2], earlier[2])
    final_doc = jnp.where(later[3] < 0.0, earlier[3], later[3])
    return (decay_total, state_total, first_doc, final_doc)


def rms_rows(rows, gain):
    wide = rows.astype(jnp.float32)
    return (wide * lax.rsqrt(jnp.mean(wide * wide, axis=-1, keepdims=True) + eps) * gain).astype(
        jnp.bfloat16
    )


def per_device(
    skip_connection_stream,
    probing_vectors,
    addressing_vectors,
    mapped_payloads,
    emission_switch,
    lapse_preactivation,
    lapse_shift_entries,
    surplus_attenuation_terms,
    passage_label_per_token,
    attention_group_rescaler,
    emission_projector,
    perceptron_rescaler,
    switching_projector,
    widening_projector,
    shrinking_projector,
):
    gate_full, up_full = sent_together((switching_projector, widening_projector), SP, 0, 1)
    down_full = whole_of(shrinking_projector, SP, (1, 0, 2), 1)
    rows_here = skip_connection_stream.shape[0]
    heads_here = probing_vectors.shape[1] // DK
    keeping_exponent = (
        jax.nn.log_sigmoid(lapse_preactivation.astype(jnp.float32) + lapse_shift_entries[None, :])
        / sharpness_factor
        + surplus_attenuation_terms[:, None]
    )
    query_head_rows = head_split(probing_vectors.astype(jnp.float32) * DK ** (-0.5), heads_here)
    key_heads = head_split(addressing_vectors.astype(jnp.float32), heads_here)
    value_heads = head_split(mapped_payloads.astype(jnp.float32), heads_here)
    decay_heads = head_split(keeping_exponent, heads_here)
    zero_state = jnp.zeros((heads_here, DK, DV), jnp.float32)
    state_local, total_log, local_out, running_state = block_pass(
        query_head_rows,
        key_heads,
        value_heads,
        decay_heads,
        passage_label_per_token,
        zero_state,
        passage_label_per_token[0],
        jnp.zeros((heads_here, DK), jnp.float32),
        BLOCK,
    )
    unbroken = (passage_label_per_token[0] == passage_label_per_token[-1]).astype(jnp.float32)
    summary = (
        jnp.exp(total_log) * unbroken,
        state_local,
        passage_label_per_token[0].astype(jnp.float32),
        passage_label_per_token[-1].astype(jnp.float32),
    )
    identity = (
        jnp.ones_like(total_log),
        jnp.zeros_like(state_local),
        jnp.full((), -1.0, jnp.float32),
        jnp.full((), -1.0, jnp.float32),
    )
    carried_state = carried_in(summary, SP, join_spans, identity)
    reaches = (passage_label_per_token.astype(jnp.float32) == carried_state[3]).astype(jnp.float32)
    incoming = (
        jnp.einsum("qlj,qjf->qlf", query_head_rows * jnp.exp(running_state), carried_state[1])
        * reaches[None, :, None]
    )
    attn = local_out + incoming
    normed_attn = (
        attn
        * lax.rsqrt(jnp.mean(attn * attn, axis=-1, keepdims=True) + eps)
        * attention_group_rescaler
    )
    flat = normed_attn.transpose(1, 0, 2).reshape(rows_here, heads_here * DV)
    gated = (flat * jax.nn.silu(emission_switch.astype(jnp.float32))).astype(jnp.bfloat16)
    share_rows = rows_here // lax.axis_size("tp")
    own_start = lax.axis_index("tp") * share_rows
    mixed = lax.psum(
        jnp.dot(gated, emission_projector, preferred_element_type=jnp.float32).astype(jnp.bfloat16),
        "tp",
    ).astype(jnp.float32)
    first_all = (skip_connection_stream.astype(jnp.float32) + mixed).astype(jnp.bfloat16)
    normed = rms_rows(first_all, perceptron_rescaler)
    first_own = lax.dynamic_slice_in_dim(first_all, own_start, share_rows, 0)
    gate = jnp.dot(normed, gate_full, preferred_element_type=jnp.float32)
    upper = jnp.dot(normed, up_full, preferred_element_type=jnp.float32)
    hidden = (jax.nn.silu(gate) * upper).astype(jnp.bfloat16)
    terms = jnp.dot(hidden, down_full, preferred_element_type=jnp.float32)
    ffn_out = sum_at_owner(terms.astype(jnp.bfloat16), "tp", 0)
    return (first_own.astype(jnp.float32) + 0.5 * ffn_out).astype(jnp.bfloat16)


def solution(mesh):
    torus = Mesh(mesh.devices.reshape(8, 4, 2, mesh.shape["tp"]), ("sp_0", "sp_1", "sp_2", "tp"))
    in_specs = (
        P(SP, None),
        P(SP, "tp"),
        P(SP, "tp"),
        P(SP, "tp"),
        P(SP, "tp"),
        P(SP, "tp"),
        P("tp"),
        P(SP),
        P(SP),
        P(),
        P("tp", None),
        P(),
        P(SP, "tp"),
        P(SP, "tp"),
        P("tp", SP),
    )
    out_specs = P(SP_TP, None)
    return jax.shard_map(
        per_device, mesh=torus, in_specs=in_specs, out_specs=out_specs, check_vma=False
    )
```

profile of v0, /device:TPU:1, one launch (start us, length us, event | category | flops | bytes accessed | tf_op | source)
XLA Modules:
  0.0 421.3 jit_solution(692808339452739212)
XLA Ops:
  7.4 11.8 %all-gather.3 = bf16[5632,32]{0,1:T(8,128)(2,1)S(1)} all-gather(bf16[1408,32]{0,1:T(8,128)(2,1)} %param.31), channel_id=5, replica_groups=mesh['sp_0'=8,'sp_1'=4,'sp_2'=2,'tp'=4] {'sp_1'}, dimensions={0}, use_global_device_ids=true | all-gather | bytes 450560 | tf_op jit(solution)/shard_map/all_gather | solution.py:36
  20.1 1.3 fusion.170
  27.9 1.2 copy.75
  31.1 1.2 reshape.743
  32.3 1.3 reshape.835
  33.5 1.3 reshape.750
  34.8 90.2 %while.19 = (s32[]{:T(128)}, f32[2,64,128]{2,1,0:T(8,128)S(1)}, s32[]{:T(128)}, f32[2,64]{1,0:T(2,128)S(1)}, f32[12,2,64,128]{3,2,0,1:T(8,128)}, /*index=5*/f32[...) while((s32[]{:T(128)}, f32[2,64,128]{2,1,0:T(8,128)S(1)}, ...), condition=%wide.region_2.3_spmd.clone, body=%wide.region_0.2_spmd.clone.sunk | while | flops 8065541 | bytes 1432795 | solution.py:161
  37.4 1.3 constant_dynamic-slice_fusion.7
  40.1 1.7 fusion.204
  44.9 1.3 constant_dynamic-slice_fusion.7
  47.6 1.7 fusion.204
  52.5 1.3 constant_dynamic-slice_fusion.7
  55.1 1.7 fusion.204
  60.0 1.3 constant_dynamic-slice_fusion.7
  62.6 1.7 fusion.204
  67.5 1.3 constant_dynamic-slice_fusion.7
  70.2 1.7 fusion.204
  75.0 1.3 constant_dynamic-slice_fusion.7
  77.7 1.7 fusion.204
  82.5 1.3 constant_dynamic-slice_fusion.7
  85.2 1.7 fusion.204
  90.1 1.3 constant_dynamic-slice_fusion.7
  92.7 1.7 fusion.204
  97.6 1.3 constant_dynamic-slice_fusion.7
  100.2 1.7 fusion.204
  105.1 1.3 constant_dynamic-slice_fusion.7
  107.7 1.7 fusion.204
  112.6 1.3 constant_dynamic-slice_fusion.7
  115.3 1.7 fusion.204
  120.1 1.3 constant_dynamic-slice_fusion.7
  122.8 1.7 fusion.204
  125.2 6.0 %all-gather.6 = bf16[2,131,128]{2,1,0:T(8,128)(2,1)S(1)} all-gather(bf16[1,131,128]{2,1,0:T(8,128)(2,1)S(1)} %maximum_bitcast_fusion), channel_id=2, replica_groups=mesh['sp_0'=8,'sp_1'=4,'sp_2'=2,'tp'=4] {'sp_2'}, dimensions={0}, use_global_device_ids=true | all-gather | bytes 100608 | tf_op jit(solution)/shard_map/all_gather | solution.py:61
  139.1 9.1 %all-gather.7 = bf16[4,131,128]{2,1,0:T(8,128)(2,1)S(1)} all-gather(bf16[1,131,128]{2,1,0:T(8,128)(2,1)S(1)} %maximum_bitcast_fusion.1), channel_id=3, replica_groups=mesh['sp_0'=8,'sp_1'=4,'sp_2'=2,'tp'=4] {'sp_1'}, dimensions={0}, use_global_device_ids=true | all-gather | bytes 167680 | tf_op jit(solution)/shard_map/all_gather | solution.py:61
  162.2 20.9 %all-gather.8 = bf16[8,131,128]{2,1,0:T(8,128)(2,1)S(1)} all-gather(bf16[1,131,128]{2,1,0:T(8,128)(2,1)S(1)} %maximum_bitcast_fusion.2), channel_id=4, replica_groups=mesh['sp_0'=8,'sp_1'=4,'sp_2'=2,'tp'=4] {'sp_0'}, dimensions={0}, use_global_device_ids=true | all-gather | bytes 301824 | tf_op jit(solution)/shard_map/all_gather | solution.py:61
  203.2 2.3 copy.86
  206.8 1.2 exponential_bitcast_fusion
  209.8 1.8 multiply_reduce_fusion
  212.8 3.7 convolution_convert_fusion
  218.2 86.5 %all-reduce.8.cloned.1.call-done = bf16[768,2048]{1,0:T(8,128)(2,1)} async-done(((bf16[768,2048]{1,0:T(8,128)(2,1)}), bf16[768,2048]{1,0:T(8,128)(2,1)}) %all-reduce.8.cloned.1.call-update) | async-done | bytes 3145744 | tf_op jit(solution)/shard_map/psum | solution.py:265
  304.7 6.0 %fusion.36 = (f32[768]{0:T(1024)S(1)}, bf16[768,2048]{1,0:T(8,128)(2,1)}) fusion(bf16[768,2048]{1,0:T(8,128)(2,1)} %all-reduce.8.cloned.1.call-done, bf16[768,2048]{1,0:T(8,128)(2,1)} %param.17), kind=kLoop, calls=%fused_computation.48 | loop fusion | flops 11009280 | bytes 9440256 | tf_op jit(solution)/shard_map/reduce_sum | solution.py:189
  310.7 6.1 %copy.89 = bf16[8,4,2,1408,32]{3,4,2,1,0:T(8,128)(2,1)} copy(bf16[8,4,2,1408,32]{3,4,1,0,2:T(8,128)(2,1)} %bitcast.293) | data formatting | bytes 11534336 | tf_op jit(solution)/shard_map/transpose | solution.py:39
  316.9 23.4 %all-gather.13.cloned.1.call-done = bf16[2048,2816]{1,0:T(8,128)(2,1)} async-done(((bf16[32,2816]{1,0:T(8,128)(2,1)}), bf16[2048,2816]{1,0:T(8,128)(2,1)}) %all-gather.13.cloned.1.call-update) | async-done | bytes 11534352 | tf_op jit(solution)/shard_map/all_gather | solution.py:24
  340.3 9.9 %fusion.41 = f32[768,1408]{1,0:T(8,128)} fusion(bf16[2048,2816]{1,0:T(8,128)(2,1)} %all-gather.13.cloned.1.call-done, bf16[768,2048]{1,0:T(8,128)(2,1)} %get-tuple-element.199, f32[2048]{0:T(1024)S(1)} %copy-done.8, f32[768]{0:T(1024)S(1)} %add_rsqrt_fusion.1), kind=kOutput, calls=%fused_computation.55 | convolution fusion | flops 4435476480 | bytes 13249536 | tf_op jit(solution)/shard_map/dot_general | solution.py:272
  350.2 17.0 %convolution_convert_fusion.1 = bf16[768,2048]{1,0:T(8,128)(2,1)} fusion(bf16[1408,2048]{0,1:T(8,128)(2,1)} %bitcast.294, f32[768,1408]{1,0:T(8,128)} %fusion.41, bf16[2048,2816]{1,0:T(8,128)(2,1)} %all-gather.13.cloned.1.call-done, bf16[768,2048]{1,0:T(8,128)(2,1)} %get-tuple-element.199, f32[2048]{0:T(1024)S(1)} %copy-done.8, f32[768]{0:T(1024)S(1)} %add_rsqrt_fusion.1), kind=kOutput, calls=%fused_computation.59 | convolution fusion | flops 8872722432 | bytes 22162432 | tf_op jit(solution)/shard_map/dot_general | solution.py:275
  367.1 4.6 %all-to-all-start = ((bf16[4,192,2048]{2,1,0:T(8,128)(2,1)}), bf16[4,192,2048]{2,1,0:T(8,128)(2,1)}, u32[]{:S(2)}, u32[]{:S(2)}) async-start(bf16[4,192,2048]{2,1,0:T(8,128)(2,1)} %bitcast.297), calls=%async_computation | async-start | bytes 6291456 | tf_op jit(solution)/shard_map/all_to_all | solution.py:101
  371.8 37.5 %all-to-all-done = bf16[4,192,2048]{2,1,0:T(8,128)(2,1)} async-done(((bf16[4,192,2048]{2,1,0:T(8,128)(2,1)}), bf16[4,192,2048]{2,1,0:T(8,128)(2,1)}, u32[]{:S(2)}, u32[]{:S(2)}) %all-to-all-start) | async-done | bytes 3145760 | tf_op jit(solution)/shard_map/all_to_all | solution.py:101
  409.2 2.7 convert_reduce_fusion
  411.9 2.3 add_convert_fusion.1
  (268 shorter events, 57.4 us)
Async XLA Ops:
  7.4 205.4 %copy-start = (bf16[256,2048]{1,0:T(8,128)(2,1)S(1)}, bf16[256,2048]{1,0:T(8,128)(2,1)}, u32[]{:S(2)}) copy-start(bf16[256,2048]{1,0:T(8,128)(2,1)} %param.27) | copy-start | bytes 3145732
  7.4 22.6 %copy-start.6 = (f32[768]{0:T(1024)S(1)}, f32[768]{0:T(1024)}, u32[]{:S(2)}) copy-start(f32[768]{0:T(1024)} %param.24) | copy-start | bytes 9220
  7.4 22.6 %copy-start.7 = (f32[128]{0:T(128)S(1)}, f32[128]{0:T(128)}, u32[]{:S(2)}) copy-start(f32[128]{0:T(128)} %param.23) | copy-start | bytes 1540
  7.4 209.2 %all-gather.15.cloned.1.call-start = ((), (), s32[]{:S(2)}) async-start(), calls=%async_computation.3 | async-start | bytes 3244032 | tf_op jit(solution)/shard_map/all_gather | solution.py:36
  20.0 284.7 %all-reduce.8.cloned.1.call-start = ((), (), s32[]{:S(2)}) async-start(), calls=%async_computation.1 | async-start | bytes 6291456 | tf_op jit(solution)/shard_map/psum | solution.py:265
  125.1 83.8 %copy-start.5 = (s32[768]{0:T(1024)S(1)}, s32[768]{0:T(1024)}, u32[]{:S(2)}) copy-start(s32[768]{0:T(1024)} %param.25) | copy-start | bytes 9220
  183.0 23.8 %copy-start.2 = (bf16[8,131,128]{2,1,0:T(8,128)(2,1)}, bf16[8,131,128]{2,1,0:T(8,128)(2,1)S(1)}, u32[]{:S(2)}) copy-start(bf16[8,131,128]{2,1,0:T(8,128)(2,1)S(1)} %all-gather.8) | copy-start | bytes 804868
  216.5 1.0 copy-start.3
  216.5 1.0 copy-start.4
  216.5 94.2 %all-gather.17.cloned.1.call-start = ((), (), s32[]{:S(2)}) async-start(), calls=%async_computation.4 | async-start | bytes 8650752 | tf_op jit(solution)/shard_map/all_gather | solution.py:36
  217.3 123.0 %all-gather.13.cloned.1.call-start = ((), (), s32[]{:S(2)}) async-start(), calls=%async_computation.2 | async-start | bytes 11714560 | tf_op jit(solution)/shard_map/all_gather | solution.py:24
  310.7 29.5 %copy-start.8 = (f32[2048]{0:T(1024)S(1)}, f32[2048]{0:T(1024)}, u32[]{:S(2)}) copy-start(f32[2048]{0:T(1024)} %param.28) | copy-start | bytes 24580
  367.1 42.1 %all-to-all-start = ((bf16[4,192,2048]{2,1,0:T(8,128)(2,1)}), bf16[4,192,2048]{2,1,0:T(8,128)(2,1)}, u32[]{:S(2)}, u32[]{:S(2)}) async-start(bf16[4,192,2048]{2,1,0:T(8,128)(2,1)} %bitcast.297), calls=%async_computation | async-start | bytes 6291456 | tf_op jit(solution)/shard_map/all_to_all | solution.py:101
  371.8 42.4 %copy-start.1 = (bf16[256,2048]{1,0:T(8,128)(2,1)S(1)}, bf16[256,2048]{1,0:T(8,128)(2,1)}, u32[]{:S(2)}) copy-start(bf16[256,2048]{1,0:T(8,128)(2,1)} %param.27) | copy-start | bytes 3145732
Sparse Core Ops, SparseCore 0:
  20.1 45.9 all-gather.14
  219.1 29.6 all-gather.16
  251.5 88.6 all-gather.12
Sparse Core Ops, SparseCore 1:
  216.6 88.0 all-reduce.7
where the time goes:
time: 425 us; the launch traced here: 421 us
  waiting for transfers between devices  148 us (35%)
  matrix products  66.3 us (16%)
  between operations  55.1 us (13%)
  local copies, waits for them, and re-layouts  54.5 us (13%)
  blocking collectives  47.8 us (11%)
  other arithmetic  30.5 us (7%)
  loops' own time  14.1 us (3%)
  starting transfers between devices  4.94 us (1%)
    psum x1, waiting for transfers between devices, per_device(): lax.psum(jnp.dot(gated, emission_projector, preferred_element_type=jnp.fl...  86.5 us
    all_to_all x1, waiting for transfers between devices, sum_at_owner(): parts = lax.all_to_all(in_blocks(shard, dim, size), axis, 0, 0, tiled=True)  37.5 us
    all_gather x3, blocking collectives, collected_together(): both, at, found = (lax.all_gather(jnp.concatenate(lines), axis), 0, {})  36 us
    all_gather x1, waiting for transfers between devices, sent_together(): lax.all_gather(both, axis, axis=dim, tiled=True)  23.4 us
    dot_general x12, matrix products, step(): jnp.einsum('hij,hjv->hiv', scores, value_block)  20 us
    dynamic_slice x60, local copies, waits for them, and re-layouts, block_pass(): lax.scan(step, (recurrent_state, last_doc, offset), (to_blocks(query_head...  19.1 us
    dot_general x1, matrix products, per_device(): terms = jnp.dot(hidden, down_full, preferred_element_type=jnp.float32)  17 us
    another operation x1, loops' own time, block_pass(): lax.scan(step, (recurrent_state, last_doc, offset), (to_blocks(query_head...  14.1 us
  transfers between devices with their start and end apart: 5, of which 3 were waited for; matrix products, arithmetic and copies ran while one was open for 28% of the time, Pallas kernels for 0%

commit v1 on v0

v1 whole, which is shorter than its diff:
```python
import functools

import jax
import jax.numpy as jnp
from jax import lax
from jax.experimental import pallas as pl
from jax.experimental.pallas import tpu as pltpu
from jax.sharding import Mesh
from jax.sharding import PartitionSpec as P

SP = ("sp_0", "sp_1", "sp_2")
SP_TP = ("sp_0", "sp_1", "sp_2", "tp")
EPS = 1e-06
SHARP = 16.0
B = 128
LEVELS = 7
AUX = 16
REACH = 8
LAG = 4
COLS = 256
MESH = pl.DeviceIdType.MESH
F32, BF16 = jnp.float32, jnp.bfloat16


def dot(a, b):
    return lax.dot_general(a, b, (((1,), (0,)), ((), ())), preferred_element_type=F32)


def dot_nt(a, b):
    return lax.dot_general(a, b, (((1,), (1,)), ((), ())), preferred_element_type=F32)


def dot_tn(a, b):
    return lax.dot_general(a, b, (((0,), (0,)), ((), ())), preferred_element_type=F32)


def kernel(
    sizes,
    skip_ref, q_ref, k_ref, v_ref, em_ref, lapse_ref, shift_ref, sur_ref, doc_ref, again_ref,
    we_ref, fgain_ref, wg_ref, wu_ref, wd_ref,
    out_ref,
    W, We, G, first, normed, hidden, part, rbuf, sbuf, carry_r, carry_s, ssq,
    oin, qp, ub, dc, gg_ref, tree, state,
    w_recv, w_dd, w_send, e_recv, e_dd, e_send, g_recv, g_send, c_recv, c_send, r_recv, r_send,
):
    Z, X, C, Y = sizes
    NSP = Z * X * C
    K = min(REACH, NSP - 1)
    T, D = skip_ref.shape
    R, FS = wg_ref.shape
    RW = we_ref.shape[0]
    NB = T // B
    HALF = T // 2
    OWN = T // Y
    NC = D // COLS
    z, x, c, y = (lax.axis_index(a) for a in SP_TP)
    s = 1 - 2 * c
    sp = (z * X + x) * C + c
    xn, zn, yn = (x + s + X) % X, (z + s + Z) % Z, (y + s + Y) % Y
    other = 1 - c

    def spdev(i):
        return {"sp_0": i // (X * C), "sp_1": (i // C) % X, "sp_2": i % C}

    barrier = pltpu.get_barrier_semaphore()
    peers = []
    for kk in range(1, K + 1):
        peers += [spdev((sp + kk) % NSP), spdev((sp + NSP - kk) % NSP)]
    peers += [{"sp_1": (x + 1) % X}, {"sp_1": (x + X - 1) % X}]
    peers += [{"sp_0": (z + 1) % Z}, {"sp_0": (z + Z - 1) % Z}]
    peers += [{"tp": (y + 1) % Y}, {"tp": (y + Y - 1) % Y}, {"sp_2": other}]
    for peer in peers:
        pl.semaphore_signal(barrier, inc=1, device_id=peer, device_id_type=MESH)
    pl.semaphore_wait(barrier, len(peers))

    def remote(src, dst, send, recv, dev):
        return pltpu.make_async_remote_copy(
            src_ref=src, dst_ref=dst, send_sem=send, recv_sem=recv, device_id=dev, device_id_type=MESH
        )

    own_w = (wg_ref, wu_ref, wd_ref)

    def slot(m, hx, hz):
        xs = (x + X - s * hx) % X if hx else x
        zs = (z + Z - s * hz) % Z if hz else z
        row = pl.multiple_of(((zs * X + xs) * C + c) * R, R)
        return W.at[m, pl.ds(row, R), :]

    def w_pass(m, hx, hz, way):
        here = slot(m, hx, hz)
        src = own_w[m] if hx == 0 and hz == 0 else here
        if way == "x":
            remote(src, here, w_send.at[m], w_recv.at[m, hx + 1, hz], {"sp_1": xn}).start()
        elif way == "z":
            remote(src, here, w_send.at[m], w_recv.at[m, hx, hz + 1], {"sp_0": zn}).start()
        else:
            remote(src, here, w_send.at[m], w_dd.at[m], {"sp_2": other}).start()

    def w_on(m, hx, hz):
        if m == 0:
            if hz < Z - 1:
                w_pass(m, hx, hz, "z")
            if hz == 0 and hx < X - 1:
                w_pass(m, hx, hz, "x")
        else:
            if hx == 0 and hz < Z - 1:
                w_pass(m, hx, hz, "z")
            if hx < X - 1:
                w_pass(m, hx, hz, "x")
        w_pass(m, hx, hz, "d")

    def w_event(m, hx, hz):
        here = slot(m, hx, hz)
        remote(here, here, w_send.at[m], w_recv.at[m, hx, hz], {"sp_2": other}).wait_recv()
        w_on(m, hx, hz)

    WAVES = X + Z - 2 + LAG

    def wave(n):
        for m in (1, 0, 2):
            k = n - LAG if m == 2 else n
            if k == 0:
                w_on(m, 0, 0)
            if k < 1:
                continue
            for hx in range(X):
                hz = k - hx
                if 0 <= hz < Z:
                    w_event(m, hx, hz)

    EP = RW // C // 2

    def e_rows(p, h):
        yb = (y + Y - s * h) % Y if h else y
        return pl.multiple_of(yb * RW + c * (RW // C) + p * EP, EP), c * (RW // C) + p * EP

    def e_on(p, h):
        row, mine = e_rows(p, h)
        here = We.at[pl.ds(row, EP), :]
        src = we_ref.at[pl.ds(pl.multiple_of(mine, EP), EP), :] if h == 0 else here
        if h < Y - 1:
            remote(src, here, e_send, e_recv.at[p, h + 1], {"tp": yn}).start()
        if h > 0:
            remote(src, here, e_send, e_dd, {"sp_2": other}).start()

    def e_event(p, h):
        row, _ = e_rows(p, h)
        here = We.at[pl.ds(row, EP), :]
        remote(here, here, e_send, e_recv.at[p, h], {"sp_2": other}).wait_recv()
        e_on(p, h)

    def g_on(r, h):
        yb = (y + Y - s * h) % Y if h else y
        here = G.at[yb, pl.ds(r * HALF, HALF), :]
        if h < Y - 1:
            remote(here, here, g_send, g_recv.at[r, h + 1], {"tp": yn}).start()

    def g_event(r, h):
        yb = (y + Y - s * h) % Y
        here = G.at[yb, pl.ds(r * HALF, HALF), :]
        remote(here, here, g_send, g_recv.at[r, h], {"sp_2": other}).wait_recv()
        g_on(r, h)

    wave(0)
    for p in range(2):
        e_on(p, 0)
    for m in range(3):
        row = pl.multiple_of(sp * R, R)
        W[m, pl.ds(row, R), :] = own_w[m][...]
    We[pl.ds(pl.multiple_of(y * RW, RW), RW), :] = we_ref[...]

    ti = lax.broadcasted_iota(jnp.int32, (B, 2 * B), 0)
    tt = lax.broadcasted_iota(jnp.int32, (B, 2 * B), 1) & (B - 1)
    for l in range(LEVELS):
        mid = ((ti >> (l + 1)) << (l + 1)) + (1 << l) - 1
        right = ((ti >> l) & 1) == 1
        among = (right & (tt > mid) & (tt <= ti)) | (~right & (tt > ti) & (tt <= mid))
        tree[l * B : (l + 1) * B, :] = among.astype(F32).astype(BF16)
    tree[LEVELS * B : (LEVELS + 1) * B, :] = (tt <= ti).astype(F32).astype(BF16)
    tree[(LEVELS + 1) * B : (LEVELS + 2) * B, :] = (tt > ti).astype(F32).astype(BF16)

    lane2 = lax.broadcasted_iota(jnp.int32, (B, 2 * B), 1)
    chan2 = lax.broadcasted_iota(jnp.int32, (B, 2 * B), 0)
    blockdiag = ((lane2 < B) == (chan2 < B // 2)).astype(F32)
    headrow = (lax.broadcasted_iota(jnp.int32, (B, B), 0) < B // 2).astype(F32)
    headlane = (lax.broadcasted_iota(jnp.int32, (B, B), 1) < B // 2).astype(F32)

    def rows_of(b):
        return pl.ds(pl.multiple_of(b * B, B), B)

    def down(row):
        return jnp.broadcast_to(row, (B, B)).T

    def block_docs(b):
        row = doc_ref[pl.ds(b, 1), :].astype(F32)
        col = down(row)
        return row, col, col[B - 1 : B, :]

    state[...] = jnp.zeros_like(state)
    ones2 = jnp.ones((2 * B, B), BF16)

    def decay_pass(b, carried):
        total, last = carried
        rows = rows_of(b)
        pre = lapse_ref[rows, :].astype(F32) + shift_ref[...]
        soft = jnp.minimum(pre, 0.0) - jnp.log1p(jnp.exp(-jnp.abs(pre)))
        g = jnp.maximum(soft / SHARP + down(sur_ref[pl.ds(b, 1), :]), -1e4)
        hi = g.astype(BF16)
        lo = (g - hi.astype(F32)).astype(BF16)
        gg = jnp.concatenate([hi, lo], axis=0)
        gg_ref[b] = gg
        sums = dot(tree[LEVELS * B :, :], gg)
        upto, after = sums[:B], sums[B:]
        col = jnp.exp(dot_tn(gg, ones2))
        dc[b] = col
        dcol, dlast = block_docs(b)[1:]
        tail = (dcol == dlast).astype(F32)
        keys = (k_ref[rows, :].astype(F32) * jnp.exp(after) * tail).astype(BF16)
        u = dot_tn(keys, v_ref[rows, :]) * blockdiag
        ub[b] = u
        qp[rows, :] = (q_ref[rows, :].astype(F32) * (0.125 * jnp.exp(upto))).astype(BF16)
        same = (dlast == last).astype(F32)
        keep = col * same
        state[...] = state[...] * jnp.concatenate([keep, keep], axis=1) + u
        return total + upto[B - 1 : B, :], dlast

    total, last = lax.fori_loop(
        0, NB, decay_pass, (jnp.zeros((1, B), F32), jnp.full((1, B), -1.0, F32))
    )
    whole = state[...]
    carry_s[0:B, :] = (whole[:, :B] * headrow + whole[:, B:] * (1.0 - headrow)).astype(BF16)
    t_hi = total.astype(BF16).astype(F32)
    t_mid = (total - t_hi).astype(BF16).astype(F32)
    t_lo = total - t_hi - t_mid
    ri = lax.broadcasted_iota(jnp.int32, (AUX, B), 0)
    aux = jnp.where(ri == 0, t_hi, 0.0)
    aux = jnp.where(ri == 1, t_mid, aux)
    aux = jnp.where(ri == 2, t_lo, aux)
    aux = jnp.where(ri == 3, last, aux)
    carry_s[B : B + AUX, :] = aux.astype(BF16)

    ii = lax.broadcasted_iota(jnp.int32, (2 * B, B), 0) & (B - 1)
    jj = lax.broadcasted_iota(jnp.int32, (2 * B, B), 1)
    xx = ii ^ jj

    def inner_pass(b, _):
        rows = rows_of(b)
        gg = gg_ref[b]
        q = q_ref[rows, :].astype(F32) * 0.125
        key = k_ref[rows, :].astype(F32)
        qq = jnp.concatenate([q * headlane, q * (1.0 - headlane)], axis=0)
        scores = jnp.where(xx == 0, dot_nt(qq.astype(BF16), k_ref[rows, :]), 0.0)
        sums = dot(tree[: LEVELS * B, :], gg)
        for l in range(LEVELS):
            e = jnp.exp(sums[l * B : (l + 1) * B])
            sl = dot_nt((qq * jnp.concatenate([e, e], axis=0)).astype(BF16), (key * e).astype(BF16))
            mine = ((xx >> l) == 1) & (((ii >> l) & 1) == 1)
            scores = jnp.where(mine, sl, scores)
        drow, dcol = block_docs(b)[:2]
        alike = (dcol == drow).astype(F32)
        scores = scores * jnp.concatenate([alike, alike], axis=0)
        sv = dot(scores.astype(BF16), v_ref[rows, :])
        oin[rows, :] = jnp.concatenate([sv[:B, :B], sv[B:, B:]], axis=1)
        return _

    for kk in range(1, K + 1):
        remote(carry_s, carry_r.at[kk - 1], c_send, c_recv.at[kk - 1], spdev((sp + kk) % NSP)).start()

    third = max(NB * 2 // 3, 1)
    lax.fori_loop(0, third, inner_pass, 0)
    wave(1)
    e_event(0, 1)
    lax.fori_loop(third, NB, inner_pass, 0)

    for kk in range(1, K + 1):
        remote(carry_s, carry_r.at[kk - 1], c_send, c_recv.at[kk - 1], {"sp_2": other}).wait_recv()
    aux_all = jnp.concatenate([carry_r[kk, B : B + AUX, :] for kk in range(K)], axis=0)
    zi = lax.broadcasted_iota(jnp.int32, (K * AUX, B), 0)
    last_in = carry_r[0, B : B + AUX, :].astype(F32)[3:4, :]
    come = jnp.zeros((B, B), F32)
    for kk in range(1, K + 1):
        piece = carry_r[kk - 1, 0:B, :].astype(F32)
        if kk > 1:
            pick = (((zi & (AUX - 1)) < 3) & (zi < (kk - 1) * AUX)).astype(F32).astype(BF16)
            piece = piece * jnp.exp(dot_tn(aux_all, pick))
        its = carry_r[kk - 1, B : B + AUX, :].astype(F32)[3:4, :]
        good = jnp.where(its == last_in, 1.0, 0.0) * jnp.where(sp >= kk, 1.0, 0.0)
        come = come + piece * good
    state[...] = jnp.concatenate([come * headrow, come * (1.0 - headrow)], axis=1)
    last_in = jnp.where(sp >= 1, last_in, -1.0)
    e_event(1, 1)

    def outer_pass(b, last):
        rows = rows_of(b)
        dcol, dlast = block_docs(b)[1:]
        reach = (dcol == last).astype(F32)
        st = state[...]
        o = oin[rows, :] + dot(qp[rows, :], st.astype(BF16)) * jnp.concatenate([reach, reach], axis=1)
        keep = dc[b] * (dlast == last).astype(F32)
        state[...] = st * jnp.concatenate([keep, keep], axis=1) + ub[b]
        em = em_ref[rows, :].astype(F32)
        gate = em / (1.0 + jnp.exp(-em))
        halves = []
        for h in range(2):
            oh = o[:, h * B : (h + 1) * B]
            scale = lax.rsqrt(jnp.mean(oh * oh, axis=-1, keepdims=True) + EPS)
            halves.append(oh * scale * again_ref[...] * gate[:, h * B : (h + 1) * B])
        G[y, rows, :] = jnp.concatenate(halves, axis=1).astype(BF16)
        return dlast

    last = lax.fori_loop(0, NB // 2, outer_pass, last_in)
    g_on(0, 0)
    last = lax.fori_loop(NB // 2, NB, outer_pass, last)
    g_on(1, 0)

    done = [1]

    def next_wave():
        if done[0] < WAVES:
            done[0] += 1
            wave(done[0])

    next_wave()
    for h in range(1, Y):
        for r in range(2):
            if h > 1:
                e_event(r, h)
        next_wave()
        for r in range(2):
            g_event(r, h)

    remote(We.at[pl.ds(0, (Y - 1) * RW // C)], We.at[pl.ds(0, (Y - 1) * RW // C)], e_send, e_dd, {"sp_2": other}).wait_recv()
    NW = 512 if D % 512 == 0 else COLS

    def mix_half(r):
        rows = pl.ds(r * HALF, HALF)
        ssq[...] = jnp.zeros_like(ssq)

        def columns(n, _):
            cols = pl.ds(pl.multiple_of(n * NW, NW), NW)
            left = jnp.concatenate([G[yb, rows, :] for yb in range(Y)], axis=1)
            mixed = dot(left, We[:, cols])
            fr = (skip_ref[rows, cols].astype(F32) + mixed).astype(BF16)
            first[rows, cols] = fr
            wide = fr.astype(F32)
            sq = wide * wide
            ssq[...] += sum(sq[:, i * 128 : (i + 1) * 128] for i in range(NW // 128))
            return _

        lax.fori_loop(0, D // NW, columns, 0)
        ssq[...] = jnp.broadcast_to(
            lax.rsqrt(jnp.sum(ssq[...], axis=-1, keepdims=True) / D + EPS), ssq.shape
        )

        def scaled(i, _):
            mine = pl.ds(pl.multiple_of(r * HALF + i * 64, 64), 64)
            sc = ssq[pl.ds(pl.multiple_of(i * 64, 64), 64), :]
            for n in range(D // 128):
                cols = slice(n * 128, (n + 1) * 128)
                normed[mine, cols] = (first[mine, cols].astype(F32) * sc * fgain_ref[:, cols]).astype(BF16)
            return _

        lax.fori_loop(0, HALF // 64, scaled, 0)

    mix_half(0)
    next_wave()
    mix_half(1)
    while done[0] < X + Z - 2:
        next_wave()

    def all_here(m):
        n = pl.ds(0, R * X * Z)
        remote(W.at[m, n, :], W.at[m, n, :], w_send.at[m], w_dd.at[m], {"sp_2": other}).wait_recv()

    all_here(0)
    all_here(1)

    def hidden_cols(n, _):
        cols = pl.ds(pl.multiple_of(n * 128, 128), 128)
        both = dot(normed[...], jnp.concatenate([W[0, :, cols], W[1, :, cols]], axis=1))
        gate = both[:, :128]
        hidden[:, cols] = (gate / (1.0 + jnp.exp(-gate)) * both[:, 128:]).astype(BF16)
        return _

    tiles = FS // 128
    left_over = max(WAVES - done[0], 1)
    at = 0
    for i in range(left_over):
        to = tiles * (i + 1) // left_over
        lax.fori_loop(at, to, hidden_cols, 0)
        at = to
        next_wave()
    all_here(2)

    def block_of(t):
        return pl.ds(pl.multiple_of(((y + 2 * Y - s * t) % Y) * OWN, OWN), OWN)

    def send_on(t, j):
        remote(sbuf.at[t, j], rbuf.at[t, j], r_send, r_recv.at[t, j], {"tp": yn}).start()

    def arrive(t, j):
        remote(sbuf.at[t, j], rbuf.at[t, j], r_send, r_recv.at[t, j], {"sp_2": other}).wait_recv()

    def reduce_step(i, same):
        @pl.when(i < NC)
        def _():
            rows = pl.ds(pl.multiple_of(i * COLS, COLS), COLS)
            part[i] = dot_nt(hidden[...], W[2, rows, :])
            sbuf[0, i] = part[i, block_of(1), :].astype(BF16)
            send_on(0, i)

        for t in range(1, Y):
            j = i - LAG * t

            @pl.when((j >= 0) & (j < NC))
            def _():
                arrive(t - 1, j)
                total = rbuf[t - 1, j].astype(F32) + part[j, block_of(t + 1), :]
                if t < Y - 1:
                    sbuf[t, j] = total.astype(BF16)
                    send_on(t, j)
                else:
                    cols = pl.ds(pl.multiple_of(j * COLS, COLS), COLS)
                    own = first[block_of(0), cols].astype(F32)
                    out_ref[:, cols] = (own + 0.5 * total).astype(BF16)

        return same

    lax.fori_loop(0, NC + LAG * (Y - 1), reduce_step, 0)

    for m in range(3):
        n = pl.ds(0, R * (2 * X * Z - 1))
        remote(W.at[m, n, :], W.at[m, n, :], w_send.at[m], w_dd.at[m], {"sp_2": other}).wait_send()
    n = pl.ds(0, EP * 2 * 2 * (Y - 1))
    remote(We.at[n], We.at[n], e_send, e_dd, {"sp_2": other}).wait_send()
    n = pl.ds(0, Y - 1)
    remote(G.at[n], G.at[n], g_send, g_recv.at[0, 0], {"sp_2": other}).wait_send()
    n = pl.ds(0, K)
    remote(carry_r.at[n], carry_r.at[n], c_send, c_recv.at[0], {"sp_2": other}).wait_send()
    remote(sbuf, sbuf, r_send, r_recv.at[0, 0], {"sp_2": other}).wait_send()


def per_device(
    sizes,
    skip_connection_stream,
    probing_vectors,
    addressing_vectors,
    mapped_payloads,
    emission_switch,
    lapse_preactivation,
    lapse_shift_entries,
    surplus_attenuation_terms,
    passage_label_per_token,
    attention_group_rescaler,
    emission_projector,
    perceptron_rescaler,
    switching_projector,
    widening_projector,
    shrinking_projector,
):
    Z, X, C, Y = sizes
    T, D = skip_connection_stream.shape
    R, FS = switching_projector.shape
    RW = emission_projector.shape[0]
    NB = T // B
    K = min(REACH, Z * X * C - 1)
    NC = D // COLS
    operands = (
        skip_connection_stream,
        probing_vectors,
        addressing_vectors,
        mapped_payloads,
        emission_switch,
        lapse_preactivation,
        lapse_shift_entries.reshape(1, B),
        surplus_attenuation_terms.reshape(NB, B),
        passage_label_per_token.reshape(NB, B),
        attention_group_rescaler.reshape(1, B),
        emission_projector,
        perceptron_rescaler.reshape(1, D),
        switching_projector,
        widening_projector,
        shrinking_projector.T,
    )
    dma = pltpu.SemaphoreType.DMA
    return pl.pallas_call(
        functools.partial(kernel, sizes),
        out_shape=jax.ShapeDtypeStruct((T // Y, D), BF16),
        in_specs=[pl.BlockSpec(memory_space=pltpu.VMEM)] * len(operands),
        out_specs=pl.BlockSpec(memory_space=pltpu.VMEM),
        scratch_shapes=[
            pltpu.VMEM((3, D, FS), BF16),
            pltpu.VMEM((Y * RW, D), BF16),
            pltpu.VMEM((Y, T, 2 * B), BF16),
            pltpu.VMEM((T, D), BF16),
            pltpu.VMEM((T, D), BF16),
            pltpu.VMEM((T, FS), BF16),
            pltpu.VMEM((NC, T, COLS), F32),
            pltpu.VMEM((Y - 1, NC, T // Y, COLS), BF16),
            pltpu.VMEM((Y - 1, NC, T // Y, COLS), BF16),
            pltpu.VMEM((K, B + AUX, B), BF16),
            pltpu.VMEM((B + AUX, B), BF16),
            pltpu.VMEM((T // 2, 128), F32),
            pltpu.VMEM((T, 2 * B), F32),
            pltpu.VMEM((T, B), BF16),
            pltpu.VMEM((NB, B, 2 * B), F32),
            pltpu.VMEM((NB, B, B), F32),
            pltpu.VMEM((NB, 2 * B, B), BF16),
            pltpu.VMEM(((LEVELS + 2) * B, 2 * B), BF16),
            pltpu.VMEM((B, 2 * B), F32),
            dma((3, X, Z)),
            dma((3,)),
            dma((3,)),
            dma((2, Y)),
            dma(()),
            dma(()),
            dma((2, Y)),
            dma(()),
            dma((K,)),
            dma(()),
            dma((Y - 1, NC)),
            dma(()),
        ],
        compiler_params=pltpu.CompilerParams(
            collective_id=0, has_side_effects=True, vmem_limit_bytes=67043328
        ),
        name="layer",
    )(*operands)


def solution(mesh):
    sp, tp = mesh.shape["sp"], mesh.shape["tp"]
    sizes = (sp // 8, 4, 2, tp)
    torus = Mesh(mesh.devices.reshape(sizes), SP_TP)
    in_specs = (
        P(SP, None),
        P(SP, "tp"),
        P(SP, "tp"),
        P(SP, "tp"),
        P(SP, "tp"),
        P(SP, "tp"),
        P("tp"),
        P(SP),
        P(SP),
        P(),
        P("tp", None),
        P(),
        P(SP, "tp"),
        P(SP, "tp"),
        P("tp", SP),
    )
    return jax.shard_map(
        functools.partial(per_device, sizes),
        mesh=torus,
        in_specs=in_specs,
        out_specs=P(SP_TP, None),
        check_vma=False,
    )
```

time: 425 us -> 123 us (0.29)
  waiting for transfers between devices: 148 us -> 0 us
  Pallas kernels: 0 us -> 121 us
  matrix products: 66.3 us -> 0 us
  between operations: 55.1 us -> 0.01 us
  local copies, waits for them, and re-layouts: 54.5 us -> 2.09 us
  blocking collectives: 47.8 us -> 0 us
  other arithmetic: 30.5 us -> 0 us
  loops' own time: 14.1 us -> 0 us
  starting transfers between devices: 4.94 us -> 0 us
    pallas_call x0 -> x1, Pallas kernels: none -> 121 us  [per_device(): pl.pallas_call(functools.partial(kernel, sizes), out_shape=jax.ShapeDtype...]
    psum x1 -> x0, waiting for transfers between devices: 86.5 us -> none  [per_device(): lax.psum(jnp.dot(gated, emission_projector, preferred_element_type=jnp.fl...]
    dot_general x40 -> x0, matrix products: 66.3 us -> none  [the longest x12 20 us: step(): jnp.einsum('hij,hjv->hiv', scores, value_block)]
    all_gather x4 -> x0, blocking collectives: 47.8 us -> none  [the longest x3 36 us: collected_together(): both, at, found = (lax.all_gather(jnp.concatenate(lines), axis), 0, {})]
    all_to_all x1 -> x0, waiting for transfers between devices: 37.5 us -> none  [sum_at_owner(): parts = lax.all_to_all(in_blocks(shard, dim, size), axis, 0, 0, tiled=True)]
    all_gather x3 -> x0, waiting for transfers between devices: 23.4 us -> none  [the longest x1 23.4 us: sent_together(): lax.all_gather(both, axis, axis=dim, tiled=True)]
    dynamic_slice x60 -> x0, local copies, waits for them, and re-layouts: 19.1 us -> none  [block_pass(): lax.scan(step, (recurrent_state, last_doc, offset), (to_blocks(query_head...]
    another operation x1 -> x0, loops' own time: 14.1 us -> none  [block_pass(): lax.scan(step, (recurrent_state, last_doc, offset), (to_blocks(query_head...]
  transfers between devices with their start and end apart: 5 -> 0, of which waited for: 3 -> 0; matrix products, arithmetic and copies ran while one was open for 28% -> 0% of each run, Pallas kernels for 0% -> 0%
where the time goes in v1:
time: 123 us
  Pallas kernels  121 us (98%)
  local copies, waits for them, and re-layouts  2.09 us (2%)
    pallas_call x1, Pallas kernels, per_device(): pl.pallas_call(functools.partial(kernel, sizes), out_shape=jax.ShapeDtype...  121 us

profile of v1, /device:TPU:1, one launch (start us, length us, event | category | flops | bytes accessed | tf_op | source)
XLA Modules:
  0.0 123.3 jit_solution(8923418441129804547)
XLA Ops:
  0.0 121.2 %layer.1 = bf16[192,2048]{1,0:T(8,128)(2,1)} custom-call(bf16[768,2048]{1,0:T(8,128)(2,1)} %skip_ref.1, bf16[768,128]{1,0:T(8,128)(2,1)} %q_ref.1, bf16[768,128]{1,0:T(8,128)(2,1)} %k_ref.1, bf16[768,256]{1,0:T(8,128)(2,1)} %v_ref.1, bf16[768,256]{1,0:T(8,128)(2,1)} %em_ref.1, bf16[768,128]{1,0:T(8,128)(2,1)} %lapse_ref.1, f32[1,128]{1,0:T(1,128)} %bitcast.10, ...), custom_call_target="tpu_custom_call" | custom-call | tf_op jit(solution)/shard_map/layer/pallas_call | solution.py:486
  121.2 2.1 %copy.17 = bf16[192,2048]{1,0:T(8,128)(2,1)} copy(bf16[192,2048]{1,0:T(8,128)(2,1)} %layer.1) | data formatting | bytes 1572864
